TPU v7x, 32 devices: a whole 2x2x4 slice. The times are simulated.
32 devices in a mesh: sp: 8 (over z, core), tp: 4 (over y, x).
Axes of the slice: x: 2, y: 2, z: 4, core: 2. Of those that a mesh axis runs over, the one named last changes fastest.
Arguments:
- tokens: bfloat16 [1536, 4096], P('sp', 'tp'), may hold values from -60 to 60
- lean_query: bfloat16 [1536, 16, 64], P('sp', 'tp'), may hold values from -6 to 6
- lean_key: bfloat16 [1536, 2, 64], P('sp'), may hold values from -6 to 6
- lean_value: bfloat16 [1536, 2, 64], P('sp'), may hold values from -6 to 6
- lean_gains: float32 [2, 64], replicated, may hold values from 0.25 to 7.5
- broad_query: bfloat16 [1536, 16, 128], P('sp', 'tp'), may hold values from -6 to 6
- broad_key: bfloat16 [1536, 2, 128], P('sp'), may hold values from -6 to 6
- broad_value: bfloat16 [1536, 2, 128], P('sp'), may hold values from -6 to 6
- broad_gains: float32 [2, 128], replicated, may hold values from 0.25 to 7.5
- mixer_gain: float32 [3072], replicated, may hold values from 0.1 to 1.9
- output_weight: bfloat16 [3072, 4096], P(None, 'tp'), may hold values from -0.109375 to 0.109375
- channel_gain: float32 [4096], P('tp'), may hold values from 0.1 to 1.9
- gate_weight: bfloat16 [8, 4096, 2048], P('sp', None, 'tp'), may hold values from -0.09375 to 0.09375
- up_weight: bfloat16 [8, 4096, 2048], P('sp', None, 'tp'), may hold values from -0.09375 to 0.09375
- down_weight: bfloat16 [8, 2048, 4096], P('sp', None, 'tp'), may hold values from -0.125 to 0.125
- route_experts: int32 [1536, 2], P('sp'), may hold values from 0 to 7, as said below
- route_logits: float32 [1536, 2], P('sp'), may hold values from -6 to 6
- group_weight: float32 [1536], P('sp'), may hold values from 0.3 to 1
Outputs:
- encoded: bfloat16 [1536, 4096], P('sp', 'tp')
Inputs may be any that keep to these rules, and one draw needn't show every extreme that they name: `route_experts`: each row names two different experts of one group, expert e lying in group e // 2. In every aligned block of 192 rows no expert is named by more than 96 rows; one group, the same for all blocks, is named by exactly half of each block's rows, and each of its experts by exactly 96 of them.
All inputs are finite; a program needn't handle non-finite values.
Results may differ from a plain program's by a relative error of at most 0.0083.
Values may be sent and summed in bfloat16 or wider, within the bound.
A program may use at most 64 MiB of HBM per device.

v0:
```python
import jax
import jax.numpy as jnp
from jax import lax
from jax.sharding import PartitionSpec as P

D = 4096
HQ_A = 16
KV_A = 2
HQ_B = 16
KV_B = 2
GRID_W = 64
GROUPS = 4
epsilon = 1e-06
theta_base = 10000.0
floor_score = -1e30


def axial_angles(positions, head_size):
    quarter = head_size // 4
    frequency = theta_base ** (-jnp.arange(quarter, dtype=jnp.float32) / quarter)
    grid_rows = (positions // GRID_W).astype(jnp.float32)
    grid_columns = (positions % GRID_W).astype(jnp.float32)
    return (grid_rows[:, None] * frequency[None, :], grid_columns[:, None] * frequency[None, :])


def turn_half(values, angles):
    half_width = values.shape[-1] // 2
    first_half = values[..., :half_width]
    second = values[..., half_width:]
    cosine = jnp.cos(angles)[:, None, :]
    sine_part = jnp.sin(angles)[:, None, :]
    return jnp.concatenate(
        [first_half * cosine - second * sine_part, second * cosine + first_half * sine_part],
        axis=-1,
    )


def prepare(raw_values, gain_row, positions):
    values = raw_values.astype(jnp.float32)
    values = (
        values * lax.rsqrt(jnp.mean(values * values, axis=-1, keepdims=True) + epsilon) * gain_row
    )
    row_angles, column_angles = axial_angles(positions, raw_values.shape[-1])
    half_width = raw_values.shape[-1] // 2
    turned = jnp.concatenate(
        [
            turn_half(values[..., :half_width], row_angles),
            turn_half(values[..., half_width:], column_angles),
        ],
        axis=-1,
    )
    return turned.astype(jnp.bfloat16)


def group_norm(head_rows, gain_row):
    values = head_rows.astype(jnp.float32)
    return (
        values * lax.rsqrt(jnp.mean(values * values, axis=-1, keepdims=True) + epsilon) * gain_row
    ).astype(jnp.bfloat16)


def own_heads(query_raw, key_raw, value_raw, gain_pair, positions, lane_index, group_ratio):
    head_count, head_size = (query_raw.shape[1], query_raw.shape[2])
    key_heads = max(1, head_count // group_ratio)
    kv_start = lane_index * head_count // group_ratio
    key_part = lax.dynamic_slice_in_dim(key_raw, kv_start, key_heads, 1)
    value_part = lax.dynamic_slice_in_dim(value_raw, kv_start, key_heads, 1)
    queries = prepare(query_raw, gain_pair[0], positions).reshape(
        query_raw.shape[0], key_heads, head_count // key_heads, head_size
    )
    return (queries, prepare(key_part, gain_pair[1], positions), value_part)


def start_state(queries):
    row_count = queries.shape[0]
    head_count = queries.shape[1] * queries.shape[2]
    return (
        jnp.full((head_count, row_count), floor_score, jnp.float32),
        jnp.zeros((head_count, row_count), jnp.float32),
        jnp.zeros((row_count, head_count, queries.shape[3]), jnp.float32),
    )


def attend_piece(fold_state, queries, keys, values):
    peak_score, weight_sum, accumulated = fold_state
    row_count, key_heads, grouped, head_size = queries.shape
    key_count = keys.shape[0]
    scores = jnp.einsum(
        "qkgd,skd->kgqs", queries, keys, preferred_element_type=jnp.float32
    ) * head_size ** (-0.5)
    scores = scores.reshape(key_heads * grouped, row_count, key_count)
    new_peak = jnp.maximum(peak_score, jnp.max(scores, axis=-1))
    weights = jnp.exp(scores - new_peak[..., None])
    new_sum = jnp.sum(weights, axis=-1)
    rounded = weights.astype(jnp.bfloat16).reshape(key_heads, grouped, row_count, key_count)
    partial_value = jnp.einsum(
        "kgqs,skd->qkgd", rounded, values, preferred_element_type=jnp.float32
    )
    partial_value = partial_value.reshape(row_count, key_heads * grouped, head_size)
    return (new_peak, new_sum, partial_value)


def finish_heads(fold_state):
    accumulated = fold_state[2]
    return (
        (accumulated / jnp.transpose(fold_state[1])[:, :, None])
        .astype(jnp.bfloat16)
        .reshape(accumulated.shape[0], -1)
    )


def on_device(
    tokens,
    lean_query,
    lean_key,
    lean_value,
    lean_gains,
    broad_query,
    broad_key,
    broad_value,
    broad_gains,
    mixer_gain,
    output_weight,
    channel_gain,
    gate_weight,
    up_weight,
    down_weight,
    route_experts,
    route_logits,
    group_weight,
):
    row_count = tokens.shape[0]
    positions = lax.axis_index("sp") * row_count + jnp.arange(row_count, dtype=jnp.int32)
    lane_index = lax.axis_index("tp")
    lean_queries, lean_keys, lean_values = own_heads(
        lean_query, lean_key, lean_value, lean_gains, positions, lane_index, HQ_A // KV_A
    )
    broad_queries, broad_keys, broad_values = own_heads(
        broad_query, broad_key, broad_value, broad_gains, positions, lane_index, HQ_B // KV_B
    )
    shard_rows = (
        lax.all_gather(lean_keys, "sp", axis=0, tiled=True),
        lax.all_gather(lean_values, "sp", axis=0, tiled=True),
        lax.all_gather(broad_keys, "sp", axis=0, tiled=True),
        lax.all_gather(broad_values, "sp", axis=0, tiled=True),
    )
    lean_state = attend_piece(start_state(lean_queries), lean_queries, shard_rows[0], shard_rows[1])
    broad_state = attend_piece(
        start_state(broad_queries), broad_queries, shard_rows[2], shard_rows[3]
    )
    lean_all, broad_all = (
        lax.all_gather(finish_heads(lean_state), "tp", axis=1, tiled=True),
        lax.all_gather(finish_heads(broad_state), "tp", axis=1, tiled=True),
    )
    lean_width = lean_all.shape[1]
    stream = tokens.astype(jnp.float32) + jnp.dot(
        group_norm(lean_all, mixer_gain[:lean_width]),
        output_weight[:lean_width],
        preferred_element_type=jnp.float32,
    )
    stream = stream + jnp.dot(
        group_norm(broad_all, mixer_gain[lean_width:]),
        output_weight[lean_width:],
        preferred_element_type=jnp.float32,
    )
    squares = lax.psum(jnp.sum(stream * stream, axis=1), "tp")
    normed = (stream * lax.rsqrt(squares / D + epsilon)[:, None] * channel_gain).astype(
        jnp.bfloat16
    )
    experts = lax.axis_size("sp")
    capacity = row_count // (experts // GROUPS)
    flat_experts = route_experts.reshape(-1)
    onehot = (flat_experts[:, None] == jnp.arange(experts, dtype=jnp.int32)[None, :]).astype(
        jnp.int32
    )
    slot_rank = jnp.sum((jnp.cumsum(onehot, axis=0) - 1) * onehot, axis=1)
    slot_index = flat_experts * capacity + slot_rank
    token_owner = jnp.repeat(jnp.arange(row_count, dtype=jnp.int32), route_experts.shape[1])
    filled = jnp.zeros((experts * capacity,), jnp.int32).at[slot_index].set(token_owner + 1)
    slot_live = (filled > 0)[:, None]
    source = jnp.maximum(filled - 1, 0)
    outgoing = jnp.where(slot_live, normed[source], jnp.zeros((), jnp.bfloat16)).reshape(
        experts, capacity, -1
    )
    arrived = lax.all_to_all(outgoing, "sp", split_axis=0, concat_axis=0, tiled=True)
    sources = arrived.shape[0]
    item_count = arrived.shape[1]
    shard_rows = lax.all_gather(arrived, "tp", axis=2, tiled=True)
    flat_rows = shard_rows.reshape(sources * item_count, shard_rows.shape[2])
    gate_part = gate_weight[0]
    up_part = up_weight[0]
    gate_value = jnp.dot(flat_rows, gate_part, preferred_element_type=jnp.float32)
    up_value = jnp.dot(flat_rows, up_part, preferred_element_type=jnp.float32)
    hidden = (jax.nn.silu(gate_value) * up_value).astype(jnp.bfloat16)
    down_part = down_weight[0]
    result = jnp.dot(
        lax.all_gather(hidden, "tp", axis=1, tiled=True),
        down_part,
        preferred_element_type=jnp.float32,
    )
    result = result.astype(jnp.bfloat16).reshape(sources, item_count, -1)
    returned = lax.all_to_all(result, "sp", split_axis=0, concat_axis=0, tiled=True)
    picked = (
        returned.reshape(experts * capacity, -1)[slot_index]
        .reshape(row_count, route_experts.shape[1], -1)
        .astype(jnp.float32)
    )
    logit_gap = route_logits[:, 0] - route_logits[:, 1]
    weights = group_weight[:, None] * jax.nn.sigmoid(jnp.stack([logit_gap, -logit_gap], axis=1))
    return (stream + jnp.sum(picked * weights[:, :, None], axis=1)).astype(jnp.bfloat16)


def solution(mesh):
    return jax.shard_map(
        on_device,
        mesh=mesh,
        in_specs=(
            P("sp", "tp"),
            P("sp", "tp", None),
            P("sp", None, None),
            P("sp", None, None),
            P(),
            P("sp", "tp", None),
            P("sp", None, None),
            P("sp", None, None),
            P(),
            P(),
            P(None, "tp"),
            P("tp"),
            P("sp", None, "tp"),
            P("sp", None, "tp"),
            P("sp", None, "tp"),
            P("sp", None),
            P("sp", None),
            P("sp"),
        ),
        out_specs=P("sp", "tp"),
        check_vma=False,
    )
```

profile of v0, /device:TPU:0, one launch (start us, length us, event | category | flops | bytes accessed | tf_op | source)
XLA Modules:
  0.0 365.0 jit_solution(18424570227048056855)
XLA Ops:
  6.6 0.8 copy.82
  7.7 0.7 broadcast_multiply_fusion
  8.4 0.9 reduce-window.6
  9.3 0.2 slice_reduce_fusion
  10.1 2.9 scatter_custom_fusion
  13.0 0.8 fusion.80
  13.8 0.8 slice_bitcast_fusion.2
  14.6 0.9 fusion.81
  16.0 17.2 %all_gather.25 = bf16[1536,1,64]{2,1,0:T(2,128)(2,1)S(1)} all-gather(bf16[192,1,64]{2,1,0:T(2,128)(2,1)S(1)} %copy.73), channel_id=1, replica_groups=mesh['sp'=8,'tp'=4] {'sp'}, dimensions={0}, use_global_device_ids=true | all-gather | bytes 221184 | tf_op jit(solution)/shard_map/all_gather | solution.py:142
  33.3 0.5 copy.74
  33.7 1.0 fusion.58
  34.7 1.0 fusion.59
  35.7 2.9 bitcast_reduce_fusion.1
  38.8 15.7 %all_gather.24 = bf16[1536,1,64]{2,1,0:T(2,128)(2,1)S(1)} all-gather(bf16[192,1,64]{2,1,0:T(2,128)(2,1)S(1)} %copy.85), channel_id=1, replica_groups=mesh['sp'=8,'tp'=4] {'sp'}, dimensions={0}, use_global_device_ids=true | all-gather | bytes 221184 | tf_op jit(solution)/shard_map/all_gather | solution.py:143
  54.5 0.5 copy.72
  55.0 3.4 fusion.3
  58.4 0.3 copy-done.1
  58.8 1.0 fusion.22
  59.8 10.3 %all_gather.26 = bf16[192,1024]{0,1:T(8,128)(2,1)S(1)} all-gather(bf16[192,256]{0,1:T(8,128)(2,1)S(1)} %fusion.60), channel_id=1, replica_groups=mesh['sp'=8,'tp'=4] {'tp'}, dimensions={1}, use_global_device_ids=true | all-gather | bytes 491520 | tf_op jit(solution)/shard_map/all_gather | solution.py:152
  70.7 0.8 multiply_cosine_fusion.1
  71.5 0.3 fusion.95
  72.0 15.2 %all_gather.28 = bf16[1536,1,128]{2,0,1:T(8,128)(2,1)S(1)} all-gather(bf16[192,1,128]{2,0,1:T(8,128)(2,1)S(1)} %copy.77), channel_id=1, replica_groups=mesh['sp'=8,'tp'=4] {'sp'}, dimensions={0}, use_global_device_ids=true | all-gather | bytes 442368 | tf_op jit(solution)/shard_map/all_gather | solution.py:144
  87.2 0.2 fusion.52
  87.6 0.4 subtract_convert_fusion.1
  88.0 1.0 bitcast_reduce_fusion
  89.1 14.6 %all_gather.27 = bf16[1536,1,128]{2,0,1:T(8,128)(2,1)S(1)} all-gather(bf16[192,1,128]{2,0,1:T(8,128)(2,1)S(1)} %copy.86), channel_id=1, replica_groups=mesh['sp'=8,'tp'=4] {'sp'}, dimensions={0}, use_global_device_ids=true | all-gather | bytes 442368 | tf_op jit(solution)/shard_map/all_gather | solution.py:145
  103.7 0.9 fusion.1
  104.6 0.9 fusion.40
  105.5 0.3 copy.79
  105.9 0.3 div.144
  106.3 12.5 %all_gather.29 = bf16[192,2048]{1,0:T(8,128)(2,1)S(1)} all-gather(bf16[192,512]{1,0:T(8,128)(2,1)S(1)} %fusion.54), channel_id=1, replica_groups=mesh['sp'=8,'tp'=4] {'tp'}, dimensions={1}, use_global_device_ids=true | all-gather | bytes 983040 | tf_op jit(solution)/shard_map/all_gather | solution.py:153
  118.7 0.2 fusion.29
  119.0 3.3 fusion.14
  122.3 2.6 multiply_reduce_fusion.1
  124.9 8.9 %psum.7 = f32[192]{0:T(256)S(1)} all-reduce(f32[192]{0:T(256)S(1)} %get-tuple-element.51), channel_id=1, replica_groups=mesh['sp'=8,'tp'=4] {'tp'}, use_global_device_ids=true, to_apply=%region_15.16 | all-reduce | flops 192 | bytes 1536 | tf_op jit(solution)/shard_map/psum | solution.py:166
  134.1 2.8 gather_fusion
  137.1 42.5 %all_to_all.10 = bf16[8,96,1024]{2,1,0:T(8,128)(2,1)} all-to-all(bf16[8,96,1024]{2,1,0:T(8,128)(2,1)S(1)} %broadcast_select_fusion), channel_id=1, replica_groups=mesh['sp'=8,'tp'=4] {'sp'}, dimensions={0} | all-to-all | bytes 3145728 | tf_op jit(solution)/shard_map/all_to_all | solution.py:185
  179.7 67.2 %all-gather.3.cloned.1.call-done = bf16[8,96,4096]{2,1,0:T(8,128)(2,1)} async-done(((bf16[8,96,1024]{2,1,0:T(8,128)(2,1)}), bf16[8,96,4096]{2,1,0:T(8,128)(2,1)}) %all-gather.3.cloned.1.call-update) | async-done | bytes 6291472 | tf_op jit(solution)/shard_map/all_gather | solution.py:188
  246.8 6.9 %fusion.12 = f32[768,512]{1,0:T(8,128)S(1)} fusion(bf16[768,4096]{1,0:T(8,128)(2,1)} %bitcast.137, bf16[1,4096,512]{2,1,0:T(8,128)(2,1)} %param.30), kind=kOutput, calls=%fused_computation.21 | convolution fusion | flops 3221225472 | bytes 12058624 | tf_op jit(solution)/shard_map/dot_general | solution.py:192
  253.9 4.4 %multiply_convert_fusion = bf16[768,512]{1,0:T(8,128)(2,1)} fusion(f32[768,512]{1,0:T(8,128)S(1)} %fusion.12, bf16[768,4096]{1,0:T(8,128)(2,1)S(1)} %bitcast.138, bf16[1,4096,512]{2,1,0:T(8,128)(2,1)S(1)} %copy-done.10), kind=kOutput, calls=%fused_computation.40 | convolution fusion | flops 3223584768 | bytes 12845056 | tf_op jit(solution)/shard_map/dot_general | solution.py:193
  258.4 43.8 %all-gather.5.cloned.1.call-done = bf16[768,2048]{1,0:T(8,128)(2,1)} async-done(((bf16[768,512]{1,0:T(8,128)(2,1)}), bf16[768,2048]{1,0:T(8,128)(2,1)}) %all-gather.5.cloned.1.call-update) | async-done | bytes 3145744 | tf_op jit(solution)/shard_map/all_gather | solution.py:197
  302.2 7.7 %fusion.26 = bf16[768,1024]{1,0:T(8,128)(2,1)} fusion(bf16[768,2048]{1,0:T(8,128)(2,1)} %all-gather.5.cloned.1.call-done, bf16[1,2048,1024]{2,1,0:T(8,128)(2,1)} %param.32), kind=kOutput, calls=%fused_computation.35 | convolution fusion | flops 3222011904 | bytes 8912896 | tf_op jit(solution)/shard_map/dot_general | solution.py:196
  309.9 4.6 %all-to-all-start.1 = ((bf16[8,96,1024]{2,1,0:T(8,128)(2,1)}), bf16[8,96,1024]{2,1,0:T(8,128)(2,1)S(1)}, u32[]{:S(2)}, u32[]{:S(2)}) async-start(bf16[8,96,1024]{2,1,0:T(8,128)(2,1)} %bitcast.131), calls=%async_computation.1 | async-start | bytes 3145728 | tf_op jit(solution)/shard_map/all_to_all | solution.py:202
  314.7 37.6 %all-to-all-done.1 = bf16[8,96,1024]{2,1,0:T(8,128)(2,1)S(1)} async-done(((bf16[8,96,1024]{2,1,0:T(8,128)(2,1)}), bf16[8,96,1024]{2,1,0:T(8,128)(2,1)S(1)}, u32[]{:S(2)}, u32[]{:S(2)}) %all-to-all-start.1) | async-done | bytes 1572896 | tf_op jit(solution)/shard_map/all_to_all | solution.py:202
  352.3 2.1 gather_fusion.1
  354.4 1.0 reshape.793
  355.4 2.0 multiply_reduce_fusion
  357.4 0.8 add_convert_fusion
  (84 shorter events, 3.6 us)
Async XLA Ops:
  6.5 63.8 %copy-start = (bf16[192,2,128]{2,1,0:T(2,128)(2,1)S(1)}, bf16[192,2,128]{2,1,0:T(2,128)(2,1)}, u32[]{:S(2)}) copy-start(bf16[192,2,128]{2,1,0:T(2,128)(2,1)} %param.24) | copy-start | bytes 294916
  6.5 240.3 %all-gather.3.cloned.1.call-start = ((), (), s32[]{:S(2)}) async-start(), calls=%async_computation.2 | async-start | bytes 7864320 | tf_op jit(solution)/shard_map/all_gather | solution.py:188
  14.6 24.1 %copy-start.4 = (bf16[192,2,64]{0,2,1:T(8,128)(2,1)S(1)}, bf16[192,2,64]{0,2,1:T(8,128)(2,1)}, u32[]{:S(2)}) copy-start(bf16[192,2,64]{0,2,1:T(8,128)(2,1)} %param.21) | copy-start | bytes 147460
  55.0 3.8 %copy-start.1 = (f32[1536,192,4]{0,1,2:T(8,128)S(1)}, f32[1536,192,4]{0,1,2:T(8,128)}, u32[]{:S(2)}) copy-start(f32[1536,192,4]{0,1,2:T(8,128)} %get-tuple-element.50) | copy-start | bytes 14155780
  58.8 11.9 %copy-start.8 = (f32[2,128]{1,0:T(2,128)S(1)}, f32[2,128]{1,0:T(2,128)}, u32[]{:S(2)}) copy-start(f32[2,128]{1,0:T(2,128)} %param.26) | copy-start | bytes 3076
  58.8 28.4 %copy-start.2 = (bf16[192,4,128]{2,1,0:T(4,128)(2,1)S(1)}, bf16[192,4,128]{2,1,0:T(4,128)(2,1)}, u32[]{:S(2)}) copy-start(bf16[192,4,128]{2,1,0:T(4,128)(2,1)} %param.23) | copy-start | bytes 589828
  87.6 1.4 copy-start.3
  104.6 14.4 %slice-start = ((f32[3072]{0:T(1024)}), f32[2048]{0:T(1024)S(1)}, s32[]{:S(2)}) async-start(f32[3072]{0:T(1024)} %param.27), calls=%async_computation.4 | async-start | bytes 16384 | tf_op jit(solution)/shard_map/slice | solution.py:162
  119.0 3.3 slice-start.1
  119.0 3.3 copy-start.11
  122.3 11.6 %copy-start.5 = (f32[1024]{0:T(1024)S(1)}, f32[1024]{0:T(1024)}, u32[]{:S(2)}) copy-start(f32[1024]{0:T(1024)} %param.29) | copy-start | bytes 12292
  179.6 122.6 %all-gather.5.cloned.1.call-start = ((), (), s32[]{:S(2)}) async-start(), calls=%async_computation.3 | async-start | bytes 3932160 | tf_op jit(solution)/shard_map/all_gather | solution.py:197
  246.8 6.9 %copy-start.9 = (bf16[8,96,4096]{2,1,0:T(8,128)(2,1)S(1)}, bf16[8,96,4096]{2,1,0:T(8,128)(2,1)}, u32[]{:S(2)}) copy-start(bf16[8,96,4096]{2,1,0:T(8,128)(2,1)} %all-gather.3.cloned.1.call-done) | copy-start | bytes 18874372
  246.8 7.0 %copy-start.10 = (bf16[1,4096,512]{2,1,0:T(8,128)(2,1)S(1)}, bf16[1,4096,512]{2,1,0:T(8,128)(2,1)}, u32[]{:S(2)}) copy-start(bf16[1,4096,512]{2,1,0:T(8,128)(2,1)} %param.31) | copy-start | bytes 12582916
  258.3 56.2 %copy-start.6 = (f32[192,2]{0,1:T(2,128)S(1)}, f32[192,2]{0,1:T(2,128)}, u32[]{:S(2)}) copy-start(f32[192,2]{0,1:T(2,128)} %param.34) | copy-start | bytes 4612
  258.4 56.2 %copy-start.7 = (f32[192]{0:T(256)S(1)}, f32[192]{0:T(256)}, u32[]{:S(2)}) copy-start(f32[192]{0:T(256)} %param.35) | copy-start | bytes 2308
  309.9 42.4 %all-to-all-start.1 = ((bf16[8,96,1024]{2,1,0:T(8,128)(2,1)}), bf16[8,96,1024]{2,1,0:T(8,128)(2,1)S(1)}, u32[]{:S(2)}, u32[]{:S(2)}) async-start(bf16[8,96,1024]{2,1,0:T(8,128)(2,1)} %bitcast.131), calls=%async_computation.1 | async-start | bytes 3145728 | tf_op jit(solution)/shard_map/all_to_all | solution.py:202
Sparse Core Ops, SparseCore 0:
  179.7 67.0 all-gather.2
  258.5 43.7 all-gather.4
where the time goes:
time: 366 us; the launch traced here: 365 us
  waiting for transfers between devices  149 us (41%)
  blocking collectives  137 us (37%)
  matrix products  30.7 us (8%)
  other arithmetic  15.9 us (4%)
  local copies, waits for them, and re-layouts  14.3 us (4%)
  between operations  13.9 us (4%)
  starting transfers between devices  4.65 us (1%)
    all_gather x1, waiting for transfers between devices, on_device(): shard_rows = lax.all_gather(arrived, 'tp', axis=2, tiled=True)  67.2 us
    all_gather x1, waiting for transfers between devices, on_device(): lax.all_gather(hidden, 'tp', axis=1, tiled=True)  43.8 us
    all_to_all x1, blocking collectives, on_device(): lax.all_to_all(outgoing, 'sp', split_axis=0, concat_axis=0, tiled=True)  42.5 us
    all_to_all x1, waiting for transfers between devices, on_device(): lax.all_to_all(result, 'sp', split_axis=0, concat_axis=0, tiled=True)  37.6 us
    all_gather x1, blocking collectives, on_device(): lax.all_gather(lean_keys, 'sp', axis=0, tiled=True)  17.2 us
    all_gather x1, blocking collectives, on_device(): lax.all_gather(lean_values, 'sp', axis=0, tiled=True)  15.7 us
    all_gather x1, blocking collectives, on_device(): lax.all_gather(broad_keys, 'sp', axis=0, tiled=True)  15.2 us
    all_gather x1, blocking collectives, on_device(): lax.all_gather(broad_values, 'sp', axis=0, tiled=True)  14.6 us
  transfers between devices with their start and end apart: 3, of which 3 were waited for; matrix products, arithmetic and copies ran while one was open for 0% of the time, Pallas kernels for 0%

commit v1 on v0

--- a/solution.py
+++ b/solution.py
@@ -194,7 +194,7 @@
     hidden = (jax.nn.silu(gate_value) * up_value).astype(jnp.bfloat16)
     down_part = down_weight[0]
     result = jnp.dot(
-        lax.all_gather(hidden, "tp", axis=1, tiled=True),
+        jnp.concatenate(lax.all_gather(hidden, "tp"), axis=1),
         down_part,
         preferred_element_type=jnp.float32,
     )

time: 366 us -> 368 us (level)
  no operation moved by 1% of the time
where the time goes in v1:
time: 368 us; the launch traced here: 367 us
  waiting for transfers between devices  149 us (40%)
  blocking collectives  137 us (37%)
  matrix products  29.8 us (8%)
  local copies, waits for them, and re-layouts  17.4 us (5%)
  other arithmetic  15.9 us (4%)
  between operations  14 us (4%)
  starting transfers between devices  4.65 us (1%)
    all_gather x1, waiting for transfers between devices, on_device(): shard_rows = lax.all_gather(arrived, 'tp', axis=2, tiled=True)  67.2 us
    all_gather x1, waiting for transfers between devices, on_device(): lax.all_gather(hidden, 'tp')  44 us
    all_to_all x1, blocking collectives, on_device(): lax.all_to_all(outgoing, 'sp', split_axis=0, concat_axis=0, tiled=True)  42.5 us
    all_to_all x1, waiting for transfers between devices, on_device(): lax.all_to_all(result, 'sp', split_axis=0, concat_axis=0, tiled=True)  37.6 us
    all_gather x1, blocking collectives, on_device(): lax.all_gather(lean_keys, 'sp', axis=0, tiled=True)  17.2 us
    all_gather x1, blocking collectives, on_device(): lax.all_gather(lean_values, 'sp', axis=0, tiled=True)  15.7 us
    all_gather x1, blocking collectives, on_device(): lax.all_gather(broad_keys, 'sp', axis=0, tiled=True)  15.2 us
    all_gather x1, blocking collectives, on_device(): lax.all_gather(broad_values, 'sp', axis=0, tiled=True)  14.6 us
  transfers between devices with their start and end apart: 3, of which 3 were waited for; matrix products, arithmetic and copies ran while one was open for 0% of the time, Pallas kernels for 0%

profile of v1, /device:TPU:0, one launch (start us, length us, event | category | flops | bytes accessed | tf_op | source)
XLA Modules:
  0.0 367.5 jit_solution(12655187102122405816)
XLA Ops:
  6.6 0.8 copy.86
  7.7 0.7 broadcast_multiply_fusion
  8.4 0.9 reduce-window.6
  10.1 2.9 scatter_custom_fusion
  13.0 0.8 fusion.80
  13.8 0.8 slice_bitcast_fusion.2
  14.6 0.9 fusion.81
  16.0 17.2 %all_gather.28 = bf16[1536,1,64]{2,1,0:T(2,128)(2,1)S(1)} all-gather(bf16[192,1,64]{2,1,0:T(2,128)(2,1)S(1)} %copy.77), channel_id=1, replica_groups=mesh['sp'=8,'tp'=4] {'sp'}, dimensions={0}, use_global_device_ids=true | all-gather | bytes 221184 | tf_op jit(solution)/shard_map/all_gather | solution.py:142
  33.3 0.5 copy.78
  33.7 1.0 fusion.58
  34.7 1.0 fusion.59
  35.7 2.9 bitcast_reduce_fusion.1
  38.8 15.7 %all_gather.27 = bf16[1536,1,64]{2,1,0:T(2,128)(2,1)S(1)} all-gather(bf16[192,1,64]{2,1,0:T(2,128)(2,1)S(1)} %copy.90), channel_id=1, replica_groups=mesh['sp'=8,'tp'=4] {'sp'}, dimensions={0}, use_global_device_ids=true | all-gather | bytes 221184 | tf_op jit(solution)/shard_map/all_gather | solution.py:143
  54.5 0.5 copy.76
  55.0 3.4 fusion.3
  58.4 0.3 copy-done.2
  58.8 1.0 fusion.22
  59.8 10.3 %all_gather.29 = bf16[192,1024]{0,1:T(8,128)(2,1)S(1)} all-gather(bf16[192,256]{0,1:T(8,128)(2,1)S(1)} %fusion.60), channel_id=1, replica_groups=mesh['sp'=8,'tp'=4] {'tp'}, dimensions={1}, use_global_device_ids=true | all-gather | bytes 491520 | tf_op jit(solution)/shard_map/all_gather | solution.py:152
  70.7 0.8 multiply_cosine_fusion.1
  71.5 0.3 fusion.95
  72.0 15.2 %all_gather.31 = bf16[1536,1,128]{2,0,1:T(8,128)(2,1)S(1)} all-gather(bf16[192,1,128]{2,0,1:T(8,128)(2,1)S(1)} %copy.81), channel_id=1, replica_groups=mesh['sp'=8,'tp'=4] {'sp'}, dimensions={0}, use_global_device_ids=true | all-gather | bytes 442368 | tf_op jit(solution)/shard_map/all_gather | solution.py:144
  87.2 0.2 fusion.52
  87.6 0.4 subtract_convert_fusion.1
  88.0 1.0 bitcast_reduce_fusion
  89.1 14.6 %all_gather.30 = bf16[1536,1,128]{2,0,1:T(8,128)(2,1)S(1)} all-gather(bf16[192,1,128]{2,0,1:T(8,128)(2,1)S(1)} %copy.91), channel_id=1, replica_groups=mesh['sp'=8,'tp'=4] {'sp'}, dimensions={0}, use_global_device_ids=true | all-gather | bytes 442368 | tf_op jit(solution)/shard_map/all_gather | solution.py:145
  103.7 0.9 fusion.1
  104.6 0.9 fusion.40
  105.5 0.3 copy.83
  105.9 0.3 div.144
  106.3 12.5 %all_gather.32 = bf16[192,2048]{1,0:T(8,128)(2,1)S(1)} all-gather(bf16[192,512]{1,0:T(8,128)(2,1)S(1)} %fusion.54), channel_id=1, replica_groups=mesh['sp'=8,'tp'=4] {'tp'}, dimensions={1}, use_global_device_ids=true | all-gather | bytes 983040 | tf_op jit(solution)/shard_map/all_gather | solution.py:153
  118.7 0.2 fusion.29
  119.0 3.3 fusion.14
  122.3 2.6 multiply_reduce_fusion.1
  124.9 8.9 %psum.7 = f32[192]{0:T(256)S(1)} all-reduce(f32[192]{0:T(256)S(1)} %get-tuple-element.51), channel_id=1, replica_groups=mesh['sp'=8,'tp'=4] {'tp'}, use_global_device_ids=true, to_apply=%region_15.16 | all-reduce | flops 192 | bytes 1536 | tf_op jit(solution)/shard_map/psum | solution.py:166
  134.1 2.8 gather_fusion
  137.1 42.5 %all_to_all.10 = bf16[8,96,1024]{2,1,0:T(8,128)(2,1)} all-to-all(bf16[8,96,1024]{2,1,0:T(8,128)(2,1)S(1)} %broadcast_select_fusion), channel_id=1, replica_groups=mesh['sp'=8,'tp'=4] {'sp'}, dimensions={0} | all-to-all | bytes 3145728 | tf_op jit(solution)/shard_map/all_to_all | solution.py:185
  179.7 67.2 %all-gather.4.cloned.1.call-done = bf16[8,96,4096]{2,1,0:T(8,128)(2,1)} async-done(((bf16[8,96,1024]{2,1,0:T(8,128)(2,1)}), bf16[8,96,4096]{2,1,0:T(8,128)(2,1)}) %all-gather.4.cloned.1.call-update) | async-done | bytes 6291472 | tf_op jit(solution)/shard_map/all_gather | solution.py:188
  246.9 6.9 %fusion.12 = f32[768,512]{1,0:T(8,128)S(1)} fusion(bf16[768,4096]{1,0:T(8,128)(2,1)} %bitcast.143, bf16[1,4096,512]{2,1,0:T(8,128)(2,1)} %param.30), kind=kOutput, calls=%fused_computation.21 | convolution fusion | flops 3221225472 | bytes 12058624 | tf_op jit(solution)/shard_map/dot_general | solution.py:192
  253.9 4.4 %multiply_convert_fusion = bf16[768,512]{1,0:T(8,128)(2,1)} fusion(f32[768,512]{1,0:T(8,128)S(1)} %fusion.12, bf16[768,4096]{1,0:T(8,128)(2,1)S(1)} %bitcast.144, bf16[1,4096,512]{2,1,0:T(8,128)(2,1)S(1)} %copy-done.13), kind=kOutput, calls=%fused_computation.40 | convolution fusion | flops 3223584768 | bytes 12845056 | tf_op jit(solution)/shard_map/dot_general | solution.py:193
  258.4 44.0 %all-gather.6.cloned.1.call-done = bf16[3072,512]{1,0:T(8,128)(2,1)} async-done(((bf16[768,512]{1,0:T(8,128)(2,1)}), bf16[3072,512]{1,0:T(8,128)(2,1)}) %all-gather.6.cloned.1.call-update) | async-done | bytes 3145744 | tf_op jit(solution)/shard_map/all_gather | solution.py:197
  302.4 3.2 copy.88
  305.6 6.8 %fusion.26 = bf16[768,1024]{1,0:T(8,128)(2,1)} fusion(bf16[768,2048]{0,1:T(8,128)(2,1)S(1)} %bitcast.136, bf16[1,2048,1024]{2,1,0:T(8,128)(2,1)} %param.32), kind=kOutput, calls=%fused_computation.35 | convolution fusion | flops 3222011904 | bytes 8912896 | tf_op jit(solution)/shard_map/dot_general | solution.py:196
  312.3 4.6 %all-to-all-start.1 = ((bf16[8,96,1024]{2,1,0:T(8,128)(2,1)}), bf16[8,96,1024]{2,1,0:T(8,128)(2,1)S(1)}, u32[]{:S(2)}, u32[]{:S(2)}) async-start(bf16[8,96,1024]{2,1,0:T(8,128)(2,1)} %bitcast.137), calls=%async_computation.1 | async-start | bytes 3145728 | tf_op jit(solution)/shard_map/all_to_all | solution.py:202
  317.2 37.6 %all-to-all-done.1 = bf16[8,96,1024]{2,1,0:T(8,128)(2,1)S(1)} async-done(((bf16[8,96,1024]{2,1,0:T(8,128)(2,1)}), bf16[8,96,1024]{2,1,0:T(8,128)(2,1)S(1)}, u32[]{:S(2)}, u32[]{:S(2)}) %all-to-all-start.1) | async-done | bytes 1572896 | tf_op jit(solution)/shard_map/all_to_all | solution.py:202
  354.8 2.1 gather_fusion.1
  356.8 1.0 reshape.801
  357.8 2.0 multiply_reduce_fusion
  359.8 0.8 add_convert_fusion
  (91 shorter events, 3.9 us)
Async XLA Ops:
  6.5 63.8 %copy-start = (bf16[192,2,128]{2,1,0:T(2,128)(2,1)S(1)}, bf16[192,2,128]{2,1,0:T(2,128)(2,1)}, u32[]{:S(2)}) copy-start(bf16[192,2,128]{2,1,0:T(2,128)(2,1)} %param.24) | copy-start | bytes 294916
  6.5 240.3 %all-gather.4.cloned.1.call-start = ((), (), s32[]{:S(2)}) async-start(), calls=%async_computation.2 | async-start | bytes 7864320 | tf_op jit(solution)/shard_map/all_gather | solution.py:188
  14.6 24.1 %copy-start.7 = (bf16[192,2,64]{0,2,1:T(8,128)(2,1)S(1)}, bf16[192,2,64]{0,2,1:T(8,128)(2,1)}, u32[]{:S(2)}) copy-start(bf16[192,2,64]{0,2,1:T(8,128)(2,1)} %param.21) | copy-start | bytes 147460
  55.0 3.8 %copy-start.2 = (f32[1536,192,4]{0,1,2:T(8,128)S(1)}, f32[1536,192,4]{0,1,2:T(8,128)}, u32[]{:S(2)}) copy-start(f32[1536,192,4]{0,1,2:T(8,128)} %get-tuple-element.50) | copy-start | bytes 14155780
  58.8 11.9 %copy-start.11 = (f32[2,128]{1,0:T(2,128)S(1)}, f32[2,128]{1,0:T(2,128)}, u32[]{:S(2)}) copy-start(f32[2,128]{1,0:T(2,128)} %param.26) | copy-start | bytes 3076
  58.8 28.4 %copy-start.5 = (bf16[192,4,128]{2,1,0:T(4,128)(2,1)S(1)}, bf16[192,4,128]{2,1,0:T(4,128)(2,1)}, u32[]{:S(2)}) copy-start(bf16[192,4,128]{2,1,0:T(4,128)(2,1)} %param.23) | copy-start | bytes 589828
  87.6 1.4 copy-start.6
  104.6 14.4 %slice-start = ((f32[3072]{0:T(1024)}), f32[2048]{0:T(1024)S(1)}, s32[]{:S(2)}) async-start(f32[3072]{0:T(1024)} %param.27), calls=%async_computation.4 | async-start | bytes 16384 | tf_op jit(solution)/shard_map/slice | solution.py:162
  119.0 3.3 slice-start.1
  119.0 3.3 copy-start.14
  122.3 11.6 %copy-start.8 = (f32[1024]{0:T(1024)S(1)}, f32[1024]{0:T(1024)}, u32[]{:S(2)}) copy-start(f32[1024]{0:T(1024)} %param.29) | copy-start | bytes 12292
  124.9 9.1 %copy-start.3 = (f32[192,1024]{1,0:T(8,128)}, f32[192,1024]{1,0:T(8,128)S(1)}, u32[]{:S(2)}) copy-start(f32[192,1024]{1,0:T(8,128)S(1)} %get-tuple-element.52) | copy-start | bytes 2359300
  179.6 122.7 %all-gather.6.cloned.1.call-start = ((), (), s32[]{:S(2)}) async-start(), calls=%async_computation.3 | async-start | bytes 3932160 | tf_op jit(solution)/shard_map/all_gather | solution.py:197
  246.9 6.9 %copy-start.12 = (bf16[8,96,4096]{2,1,0:T(8,128)(2,1)S(1)}, bf16[8,96,4096]{2,1,0:T(8,128)(2,1)}, u32[]{:S(2)}) copy-start(bf16[8,96,4096]{2,1,0:T(8,128)(2,1)} %all-gather.4.cloned.1.call-done) | copy-start | bytes 18874372
  246.9 7.0 %copy-start.13 = (bf16[1,4096,512]{2,1,0:T(8,128)(2,1)S(1)}, bf16[1,4096,512]{2,1,0:T(8,128)(2,1)}, u32[]{:S(2)}) copy-start(bf16[1,4096,512]{2,1,0:T(8,128)(2,1)} %param.31) | copy-start | bytes 12582916
  305.5 11.4 %copy-start.9 = (f32[192,2]{0,1:T(2,128)S(1)}, f32[192,2]{0,1:T(2,128)}, u32[]{:S(2)}) copy-start(f32[192,2]{0,1:T(2,128)} %param.34) | copy-start | bytes 4612
  305.6 11.4 %copy-start.10 = (f32[192]{0:T(256)S(1)}, f32[192]{0:T(256)}, u32[]{:S(2)}) copy-start(f32[192]{0:T(256)} %param.35) | copy-start | bytes 2308
  312.3 42.4 %all-to-all-start.1 = ((bf16[8,96,1024]{2,1,0:T(8,128)(2,1)}), bf16[8,96,1024]{2,1,0:T(8,128)(2,1)S(1)}, u32[]{:S(2)}, u32[]{:S(2)}) async-start(bf16[8,96,1024]{2,1,0:T(8,128)(2,1)} %bitcast.137), calls=%async_computation.1 | async-start | bytes 3145728 | tf_op jit(solution)/shard_map/all_to_all | solution.py:202
  354.8 5.0 %copy-start.4 = (f32[192,1024]{1,0:T(8,128)S(1)}, f32[192,1024]{1,0:T(8,128)}, u32[]{:S(2)}) copy-start(f32[192,1024]{1,0:T(8,128)} %copy-done.3) | copy-start | bytes 2359300
  354.8 5.9 %copy-start.1 = (bf16[192,2,128]{2,1,0:T(2,128)(2,1)S(1)}, bf16[192,2,128]{2,1,0:T(2,128)(2,1)}, u32[]{:S(2)}) copy-start(bf16[192,2,128]{2,1,0:T(2,128)(2,1)} %param.24) | copy-start | bytes 294916
Sparse Core Ops, SparseCore 0:
  179.7 67.0 all-gather.3
  258.5 43.8 all-gather.5
